TPU v7x, 128 devices: a whole 4x4x4 slice. The times are simulated.
128 devices in a mesh: st: 64 (over z, y, x), tp: 2 (over core).
Axes of the slice: x: 4, y: 4, z: 4, core: 2. Of those that a mesh axis runs over, the one named last changes fastest.
Arguments:
- hidden: bfloat16 [32768, 2048], P('st'), may hold values from -24 to 24
- passage_store: bfloat16 [2048, 64, 2048], P('st'), may hold values from -6 to 6
- passage_ids: int32 [512, 4], P('st'), may hold values from 0 to 2047, as said below
- query_weight: bfloat16 [2048, 512], P(None, 'tp'), may hold values from -0.125 to 0.125
- gate_weight: bfloat16 [2048, 512], P(None, 'tp'), may hold values from -0.125 to 0.125
- key_weight: bfloat16 [2048, 512], P(None, 'tp'), may hold values from -0.125 to 0.125
- value_weight: bfloat16 [2048, 512], P(None, 'tp'), may hold values from -0.125 to 0.125
- output_grad: bfloat16 [32768, 512], P('st', 'tp'), may hold values from -6 to 6
Outputs:
- grad_hidden: bfloat16 [32768, 2048], P(('st', 'tp'))
- grad_store: bfloat16 [2048, 64, 2048], P(('st', 'tp'))
- grad_value_weight: float32 [2048, 512], P(None, 'tp')
Inputs may be any that keep to these rules, and one draw needn't show every extreme that they name: `passage_ids`: passage p is held at st index p // 32. The 32 ids of one index of st (its 8 blocks) are distinct; at most 1 of them name passages of one owner, and on every index some owner is named exactly 1 times. Every index reads at least one passage of the owner before it, of the owner after it and of the owner half the axis away.
All inputs are finite; a program needn't handle non-finite values.
Results may differ from a plain program's by a relative error of at most 0.012.
The roundings to bfloat16 on the way count: a program that leaves them out, or rounds other values in their place, can miss the bound.
Values may be sent and summed in bfloat16 or wider, within the bound.
No kernel may reach another device: no remote copies, remote signals or barrier semaphores. Data moves between devices by JAX's collectives and lax.ppermute only.
A program may use at most 128 MiB of HBM per device.

v0:
```python
import functools

import jax
import jax.numpy as jnp
from jax import lax
from jax.experimental import pallas as pl
from jax.experimental.pallas import tpu as pltpu
from jax.sharding import PartitionSpec as P

HEAD_DIM = 256
PAUSE = 2650
PAUSE_AGAIN = 1300
F32 = jnp.float32
BF16 = jnp.bfloat16
VMEM = pl.BlockSpec(memory_space=pltpu.VMEM)
SMEM = pl.BlockSpec(memory_space=pltpu.SMEM)
ANY = pl.BlockSpec(memory_space=pl.ANY)


def dot(a, b, ca, cb):
    return lax.dot_general(a, b, (((ca,), (cb,)), ((), ())), preferred_element_type=F32)


def swap_tp(x):
    return lax.ppermute(x, "tp", [(0, 1), (1, 0)])


def exchange(x):
    return lax.all_to_all(x, "st", split_axis=0, concat_axis=0, tiled=True)


def request_kernel(held, ids_ref, out_ref):
    per, blocks = ids_ref.shape
    out_ref[...] = jnp.zeros_like(out_ref)
    for b in range(blocks):
        for j in range(per):
            at = ids_ref[j, b]
            owner = lax.div(at, held)
            out_ref[pl.ds(owner, 1)] = jnp.full((1, out_ref.shape[1]), at - owner * held + 1, jnp.int32)


def pick_kernel(wanted_ref, pause_ref, rows_ref, *refs):
    out_ref, wait, sem = refs[-3:]
    if pause_ref is not None:
        wait[...] = lax.fori_loop(0, pause_ref[0], lambda i, c: jnp.tanh(c), jnp.zeros(wait.shape, F32))

    def step(i, carry):
        at = jnp.maximum(wanted_ref[i, 0] - 1, 0)
        pltpu.make_async_copy(rows_ref.at[at], out_ref.at[i], sem).start()
        return carry

    lax.fori_loop(0, out_ref.shape[0], step, 0, unroll=8)
    pltpu.make_async_copy(out_ref, out_ref, sem).wait()


def pick(wanted, pause, rows, *after):
    return pl.pallas_call(
        pick_kernel,
        out_shape=jax.ShapeDtypeStruct((wanted.shape[0], *rows.shape[1:]), rows.dtype),
        in_specs=[SMEM, SMEM, VMEM] + [ANY] * len(after),
        out_specs=ANY,
        scratch_shapes=[pltpu.VMEM((8, 128), F32), pltpu.SemaphoreType.DMA],
        name="pick",
    )(wanted, pause, rows, *after)


def probs_kernel(held, ids_ref, q_ref, da_ref, k_ref, p_ref, dv_ref):
    per, blocks = ids_ref.shape
    rows = q_ref.shape[0] // blocks
    span = k_ref.shape[1]
    scale = HEAD_DIM**-0.5
    for b in range(blocks):
        mine = slice(b * rows, (b + 1) * rows)
        owner = [lax.div(ids_ref[j, b], held) for j in range(per)]
        k = jnp.concatenate([k_ref[o] for o in owner], axis=0)
        s = dot(q_ref[mine], k, 1, 1) * scale
        e = jnp.exp(s - jnp.max(s, axis=1, keepdims=True))
        p = e / jnp.sum(e, axis=1, keepdims=True)
        p_ref[mine] = p
        dv = dot(p.astype(BF16), da_ref[mine], 0, 0).astype(BF16)
        for j in range(per):
            dv_ref[owner[j]] = dv[j * span : (j + 1) * span]


def grads_kernel(held, ids_ref, tp_ref, q_ref, da_ref, g_ref, og_ref, p_ref, k_ref, v_ref, keep_dq, keep_dg, send_dq, send_dg, dk_ref):
    per, blocks = ids_ref.shape
    rows = q_ref.shape[0] // blocks
    span = k_ref.shape[1]
    scale = HEAD_DIM**-0.5
    half = blocks // 2
    for n in range(blocks):
        b = lax.rem(n + half * tp_ref[0], blocks)
        mine = pl.ds(pl.multiple_of(b * rows, rows), rows)
        owner = [lax.div(ids_ref[j, b], held) for j in range(per)]
        k = jnp.concatenate([k_ref[o] for o in owner], axis=0)
        v = jnp.concatenate([v_ref[o] for o in owner], axis=0)
        p = p_ref[mine]
        q = q_ref[mine]
        g = g_ref[mine]
        dp = dot(da_ref[mine], v, 1, 1)
        attended = dot(p.astype(BF16), v, 1, 0)
        centre = jnp.sum(p * dp, axis=1, keepdims=True)
        ds = (p * (dp - centre) * scale).astype(BF16)
        dq = dot(ds, k, 1, 0).astype(BF16)
        dk = dot(ds, q, 0, 0).astype(BF16)
        sg = jax.nn.sigmoid(g)
        dg = (og_ref[mine].astype(F32) * attended * sg * (1.0 + g * (1.0 - sg))).astype(BF16)
        for j in range(per):
            dk_ref[owner[j]] = dk[j * span : (j + 1) * span]
        at = slice((n % half) * rows, (n % half + 1) * rows)
        (keep_dq if n < half else send_dq)[at] = dq
        (keep_dg if n < half else send_dg)[at] = dg


def add_slots(wanted_ref, tp_ref, came_ref, acc, keep_ref, send_ref):
    acc[...] = jnp.zeros_like(acc)

    def step(i, carry):
        at = wanted_ref[i, 0]
        acc[at] = acc[at] + came_ref[i].astype(F32)
        return carry

    lax.fori_loop(0, came_ref.shape[0], step, 0, unroll=8)
    half = keep_ref.shape[0]
    tp = tp_ref[0]
    keep_ref[...] = acc[pl.ds(1 + half * tp, half)].astype(BF16)
    send_ref[...] = acc[pl.ds(1 + half * (1 - tp), half)].astype(BF16)


def add_slots_kernel(wanted_ref, tp_ref, came_ref, keep_ref, send_ref, acc):
    add_slots(wanted_ref, tp_ref, came_ref, acc, keep_ref, send_ref)


def value_totals_kernel(wanted_ref, tp_ref, came_ref, keep_ref, send_ref, all_ref, acc):
    add_slots(wanted_ref, tp_ref, came_ref, acc, keep_ref, send_ref)
    held, span = acc.shape[0] - 1, acc.shape[1]
    for i in range(held):
        all_ref[:, i * span : (i + 1) * span] = acc[1 + i].T.astype(BF16)


def weight_kernel(store_ref, vt_ref, out_ref):
    part = dot(vt_ref[...], store_ref[...], 1, 0).T.astype(BF16)
    rows = out_ref.shape[1]
    for i in range(out_ref.shape[0]):
        out_ref[i] = part[i * rows : (i + 1) * rows]


def back_kernel(terms, *refs):
    out_ref = refs[-1]
    a = jnp.concatenate([r[...] for r in refs[:terms]], axis=1)
    step = 256
    for n in range(0, out_ref.shape[1], step):
        w = jnp.concatenate([r[n : n + step] for r in refs[terms:-1]], axis=1)
        out_ref[:, n : n + step] = dot(a, w, 1, 1).astype(out_ref.dtype)


def back(terms, weights, dtype, tile=256):
    rows, width = terms[0].shape
    depth = weights[0].shape[0]
    return pl.pallas_call(
        functools.partial(back_kernel, len(terms)),
        grid=(rows // tile,),
        out_shape=jax.ShapeDtypeStruct((rows, depth), dtype),
        in_specs=[pl.BlockSpec((tile, width), lambda i: (i, 0))] * len(terms)
        + [pl.BlockSpec((depth, width), lambda i: (0, 0))] * len(weights),
        out_specs=pl.BlockSpec((tile, depth), lambda i: (i, 0)),
        name="back",
    )(*terms, *weights)


def last_kernel(terms, *refs):
    one_ref, two_ref, out_ref, both_ref = refs[-4:]
    back_kernel(terms, *refs[:-4], out_ref)
    both_ref[...] = (one_ref[...] + two_ref[...].astype(F32)).astype(both_ref.dtype)


def back_and_add(terms, weights, one, two, tile=512):
    rows, width = terms[0].shape
    depth = weights[0].shape[0]
    steps = rows // tile
    thin = pl.BlockSpec((one.shape[0] // steps, depth), lambda i: (i, 0))
    wide = pl.BlockSpec((tile, depth), lambda i: (i, 0))
    return pl.pallas_call(
        functools.partial(last_kernel, len(terms)),
        grid=(steps,),
        out_shape=(jax.ShapeDtypeStruct((rows, depth), BF16), jax.ShapeDtypeStruct(one.shape, BF16)),
        in_specs=[pl.BlockSpec((tile, width), lambda i: (i, 0))] * len(terms)
        + [pl.BlockSpec((depth, width), lambda i: (0, 0))] * len(weights)
        + [thin, thin],
        out_specs=(wide, thin),
        name="last",
    )(*terms, *weights, one, two)


def body(hidden, passage_store, passage_ids, query_weight, gate_weight, key_weight, value_weight, output_grad):
    owners = lax.axis_size("st")
    held, span, depth = passage_store.shape
    _, per_block = passage_ids.shape
    width = query_weight.shape[1]
    tokens = hidden.shape[0]
    tp = lax.axis_index("tp").astype(jnp.int32).reshape(1)

    ids = passage_ids.T
    request = pl.pallas_call(
        functools.partial(request_kernel, held),
        out_shape=jax.ShapeDtypeStruct((owners, 128), jnp.int32),
        in_specs=[SMEM],
        out_specs=VMEM,
        name="request",
    )(ids)
    wanted = exchange(request)

    other_key, other_value = swap_tp(key_weight), swap_tp(value_weight)
    store_rows = passage_store.reshape(held * span, depth)
    keys = jnp.dot(store_rows, key_weight, preferred_element_type=F32).astype(BF16).reshape(held, span, width)
    pause = tp * PAUSE
    came_keys = exchange(pick(wanted, pause, keys, other_key, other_value))
    values = jnp.dot(store_rows, value_weight, preferred_element_type=F32).astype(BF16).reshape(held, span, width)
    came_values = exchange(pick(wanted, tp * PAUSE_AGAIN, values))

    queries = jnp.dot(hidden, query_weight, preferred_element_type=F32).astype(BF16)
    gates = jnp.dot(hidden, gate_weight, preferred_element_type=F32)
    d_attended = (output_grad.astype(F32) * gates * jax.nn.sigmoid(gates)).astype(BF16)

    probs, back_values = pl.pallas_call(
        functools.partial(probs_kernel, held),
        out_shape=(
            jax.ShapeDtypeStruct((tokens, per_block * span), F32),
            jax.ShapeDtypeStruct((owners, span, width), BF16),
        ),
        in_specs=[SMEM, VMEM, VMEM, VMEM],
        out_specs=(VMEM, VMEM),
        name="probs",
    )(ids, queries, d_attended, came_keys)
    came_dvalues = exchange(back_values)

    piece = depth // owners
    half_tokens = jax.ShapeDtypeStruct((tokens // 2, width), BF16)
    keep_dq, keep_dg, send_dq, send_dg, back_keys = pl.pallas_call(
        functools.partial(grads_kernel, held),
        out_shape=(half_tokens,) * 4 + (jax.ShapeDtypeStruct((owners, span, width), BF16),),
        in_specs=[SMEM, SMEM] + [VMEM] * 7,
        out_specs=(VMEM,) * 5,
        name="grads",
    )(ids, tp, queries, d_attended, gates, output_grad, probs, came_keys, came_values)

    keep_hidden = back((keep_dq, keep_dg), (query_weight, gate_weight), F32)
    send_hidden = back((send_dq, send_dg), (query_weight, gate_weight), BF16)

    half_held = jax.ShapeDtypeStruct((held // 2, span, width), BF16)
    keep_values, send_values, values_across = pl.pallas_call(
        value_totals_kernel,
        out_shape=(half_held, half_held, jax.ShapeDtypeStruct((width, held * span), BF16)),
        in_specs=[SMEM, SMEM, VMEM],
        out_specs=(VMEM, VMEM, VMEM),
        scratch_shapes=[pltpu.VMEM((held + 1, span, width), F32)],
        name="value_totals",
    )(wanted, tp, came_dvalues)

    came_dkeys = exchange(back_keys)
    tile = 256
    parts = pl.pallas_call(
        weight_kernel,
        grid=(depth // tile,),
        out_shape=jax.ShapeDtypeStruct((owners, piece, width), BF16),
        in_specs=[
            pl.BlockSpec((held * span, tile), lambda i: (0, i)),
            pl.BlockSpec((width, held * span), lambda i: (0, 0)),
        ],
        out_specs=pl.BlockSpec((tile // piece, piece, width), lambda i: (i, 0, 0)),
        name="weight",
    )(store_rows, values_across)
    came_parts = exchange(lax.optimization_barrier((parts, came_dkeys))[0])

    keep_keys, send_keys = pl.pallas_call(
        add_slots_kernel,
        out_shape=(half_held, half_held),
        in_specs=[SMEM, SMEM, VMEM],
        out_specs=(VMEM, VMEM),
        scratch_shapes=[pltpu.VMEM((held + 1, span, width), F32)],
        name="key_totals",
    )(wanted, tp, came_dkeys)
    rows = held // 2 * span
    keep_keys, send_keys, keep_values, send_values = (
        t.reshape(rows, width) for t in (keep_keys, send_keys, keep_values, send_values)
    )
    came_parts, keep_keys, send_keys = lax.optimization_barrier((came_parts, keep_keys, send_keys))
    summed = jnp.sum(came_parts.astype(F32), axis=0).astype(BF16)
    gathered = exchange(jnp.broadcast_to(summed, came_parts.shape))

    other_values = swap_tp(send_values)
    other_keys = swap_tp(send_keys)
    other_hidden = swap_tp(send_hidden)
    grad_store, grad_hidden = back_and_add(
        (keep_keys, other_keys, keep_values, other_values),
        (key_weight, other_key, value_weight, other_value),
        keep_hidden,
        other_hidden,
    )
    grad_store = grad_store.reshape(held // 2, span, depth)
    gathered, grad_hidden, grad_store = lax.optimization_barrier((gathered, grad_hidden, grad_store))
    grad_value_weight = gathered.reshape(depth, width).astype(F32)
    return grad_hidden, grad_store, grad_value_weight


def solution(mesh):
    placed = (
        P("st", None),
        P("st", None, None),
        P("st", None),
        P(None, "tp"),
        P(None, "tp"),
        P(None, "tp"),
        P(None, "tp"),
        P("st", "tp"),
    )

    return jax.shard_map(
        body,
        mesh=mesh,
        in_specs=placed,
        out_specs=(P(("st", "tp"), None), P(("st", "tp"), None, None), P(None, "tp")),
        check_vma=False,
    )
```

profile of v0, /device:TPU:0, one launch (start us, length us, event | category | flops | bytes accessed | tf_op | source)
XLA Modules:
  0.0 193.3 jit_solution(17590991992132780636)
XLA Ops:
  0.6 0.0 copy-start
  0.6 0.1 collective-permute-start
  0.7 0.5 collective-permute-start.1
  1.2 1.5 request.1
  2.8 11.5 %all-to-all-start = ((s32[64,1,128]{2,1,0:T(1,128)}), s32[64,1,128]{2,1,0:T(1,128)S(1)}, u32[]{:S(2)}, u32[]{:S(2)}) async-start(s32[64,1,128]{2,1,0:T(1,128)} %bitcast.36), calls=%async_computation | async-start | bytes 65536 | tf_op jit(solution)/shard_map/all_to_all | solution.py:29
  14.3 6.9 %convolution_convert_fusion.1 = bf16[2048,256]{1,0:T(8,128)(2,1)} fusion(bf16[2048,2048]{1,0:T(8,128)(2,1)} %bitcast.25, bf16[2048,256]{1,0:T(8,128)(2,1)} %refs_4_.1), kind=kOutput, calls=%fused_computation.1 | convolution fusion | flops 2148007936 | bytes 10485760 | tf_op jit(solution)/shard_map/dot_general | solution.py:215
  21.2 2.6 %all-to-all-done = s32[64,1,128]{2,1,0:T(1,128)S(1)} async-done(((s32[64,1,128]{2,1,0:T(1,128)}), s32[64,1,128]{2,1,0:T(1,128)S(1)}, u32[]{:S(2)}, u32[]{:S(2)}) %all-to-all-start) | async-done | bytes 32800 | tf_op jit(solution)/shard_map/all_to_all | solution.py:29
  23.8 0.0 copy-start.5
  23.8 0.0 collective-permute-done.refs_0_.refs_5_
  23.8 0.0 copy-start.3
  23.8 0.0 collective-permute-done.1.refs_1_.refs_7_
  23.8 0.6 copy-done.5
  24.4 0.5 copy-done.3
  24.9 2.5 %pick.2 = bf16[64,64,256]{2,1,0:T(8,128)(2,1)} custom-call(s32[64,128]{1,0:T(8,128)} %bitcast.30, s32[1]{0:T(128)S(6)} %mul.14.pause_ref, bf16[32,64,256]{2,1,0:T(8,128)(2,1)} %bitcast.29, bf16[2048,256]{1,0:T(8,128)(2,1)} %copy-done.3, bf16[2048,256]{1,0:T(8,128)(2,1)} %collective-permute-done.1.refs_1_.refs_7_), custom_call_target="tpu_custom_call" | custom-call | tf_op jit(solution)/shard_map/pick/pallas_call | solution.py:57
  27.4 0.0 copy-start.4
  27.4 8.2 %all-to-all-start.1 = ((bf16[64,64,256]{2,1,0:T(8,128)(2,1)}), bf16[64,64,256]{2,1,0:T(8,128)(2,1)}, u32[]{:S(2)}, u32[]{:S(2)}) async-start(bf16[64,64,256]{2,1,0:T(8,128)(2,1)} %pick.2), calls=%async_computation.1 | async-start | bytes 4194304 | tf_op jit(solution)/shard_map/all_to_all | solution.py:29
  35.6 0.0 copy-done.4
  35.6 6.7 %convolution_convert_fusion = bf16[2048,256]{1,0:T(8,128)(2,1)} fusion(bf16[2048,2048]{1,0:T(8,128)(2,1)} %bitcast.26, bf16[2048,256]{1,0:T(8,128)(2,1)S(1)} %copy-done.4), kind=kOutput, calls=%fused_computation | convolution fusion | flops 2148007936 | bytes 10485760 | tf_op jit(solution)/shard_map/dot_general | solution.py:218
  42.3 2.5 %pick.3 = bf16[64,64,256]{2,1,0:T(8,128)(2,1)} custom-call(s32[64,128]{1,0:T(8,128)} %bitcast.31, s32[1]{0:T(128)S(6)} %mul.15.pause_ref, bf16[32,64,256]{2,1,0:T(8,128)(2,1)} %bitcast.28), custom_call_target="tpu_custom_call" | custom-call | tf_op jit(solution)/shard_map/pick/pallas_call | solution.py:57
  44.9 0.0 copy-start.1
  44.9 11.5 %all-to-all-done.1.k_ref = bf16[64,64,256]{2,1,0:T(8,128)(2,1)} async-done(((bf16[64,64,256]{2,1,0:T(8,128)(2,1)}), bf16[64,64,256]{2,1,0:T(8,128)(2,1)}, u32[]{:S(2)}, u32[]{:S(2)}) %all-to-all-start.1) | async-done | bytes 2097184 | tf_op jit(solution)/shard_map/all_to_all | solution.py:29
  56.4 5.6 %all-to-all-start.3 = ((bf16[64,64,256]{2,1,0:T(8,128)(2,1)}), bf16[64,64,256]{2,1,0:T(8,128)(2,1)}, u32[]{:S(2)}, u32[]{:S(2)}) async-start(bf16[64,64,256]{2,1,0:T(8,128)(2,1)} %pick.3), calls=%async_computation.3 | async-start | bytes 4194304 | tf_op jit(solution)/shard_map/all_to_all | solution.py:29
  62.0 0.0 copy-done
  62.0 0.0 copy-done.1
  62.0 0.0 copy-start.2
  62.0 0.0 copy-start.6
  62.0 1.4 convolution_convert_fusion.2.q_ref
  63.5 0.0 copy-done.2
  63.5 0.0 copy-done.6
  63.5 1.6 multiply_convert_fusion
  65.1 5.4 %probs.1 = (f32[512,256]{1,0:T(8,128)}, bf16[64,64,256]{2,1,0:T(8,128)(2,1)}) custom-call(s32[4,8]{1,0:T(4,128)} %bitcast.38, bf16[512,256]{1,0:T(8,128)(2,1)} %convolution_convert_fusion.2.q_ref, bf16[512,256]{1,0:T(8,128)(2,1)} %get-tuple-element.45.da_ref, bf16[64,64,256]{2,1,0:T(8,128)(2,1)} %all-to-all-done.1.k_ref), custom_call_target="tpu_custom_call" | custom-call | tf_op jit(solution)/shard_map/probs/pallas_call | solution.py:225
  70.5 12.3 %all-to-all-done.3.v_ref = bf16[64,64,256]{2,1,0:T(8,128)(2,1)} async-done(((bf16[64,64,256]{2,1,0:T(8,128)(2,1)}), bf16[64,64,256]{2,1,0:T(8,128)(2,1)}, u32[]{:S(2)}, u32[]{:S(2)}) %all-to-all-start.3) | async-done | bytes 2097184 | tf_op jit(solution)/shard_map/all_to_all | solution.py:29
  82.8 5.7 %all-to-all-start.2 = ((bf16[64,64,256]{2,1,0:T(8,128)(2,1)}), bf16[64,64,256]{2,1,0:T(8,128)(2,1)}, u32[]{:S(2)}, u32[]{:S(2)}) async-start(bf16[64,64,256]{2,1,0:T(8,128)(2,1)} %get-tuple-element.24), calls=%async_computation.2 | async-start | bytes 4194304 | tf_op jit(solution)/shard_map/all_to_all | solution.py:29
  88.6 6.8 %grads.1 = (bf16[256,256]{1,0:T(8,128)(2,1)}, bf16[256,256]{1,0:T(8,128)(2,1)}, bf16[256,256]{1,0:T(8,128)(2,1)}, bf16[256,256]{1,0:T(8,128)(2,1)}, bf16[64,64,256]{2,1,0:T(8,128)(2,1)}) custom-call(s32[4,8]{1,0:T(4,128)} %bitcast.39, s32[1]{0:T(128)} %bitcast.5.tp_ref, bf16[512,256]{1,0:T(8,128)(2,1)} %convolution_convert_fusion.2.q_ref, ...), custom_call_target="tpu_custom_call" | custom-call | tf_op jit(solution)/shard_map/grads/pallas_call | solution.py:239
  95.3 14.3 %all-to-all-done.2.came_ref = bf16[64,64,256]{2,1,0:T(8,128)(2,1)} async-done(((bf16[64,64,256]{2,1,0:T(8,128)(2,1)}), bf16[64,64,256]{2,1,0:T(8,128)(2,1)}, u32[]{:S(2)}, u32[]{:S(2)}) %all-to-all-start.2) | async-done | bytes 2097184 | tf_op jit(solution)/shard_map/all_to_all | solution.py:29
  109.6 6.7 %all-to-all-start.4 = ((bf16[64,64,256]{2,1,0:T(8,128)(2,1)}), bf16[64,64,256]{2,1,0:T(8,128)(2,1)}, u32[]{:S(2)}, u32[]{:S(2)}) async-start(bf16[64,64,256]{2,1,0:T(8,128)(2,1)} %get-tuple-element.27), calls=%async_computation.4 | async-start | bytes 4194304 | tf_op jit(solution)/shard_map/all_to_all | solution.py:29
  116.3 4.7 %value_totals.1 = (bf16[16,64,256]{2,1,0:T(8,128)(2,1)}, bf16[16,64,256]{2,1,0:T(8,128)(2,1)}, bf16[256,2048]{1,0:T(8,128)(2,1)}) custom-call(s32[64,128]{1,0:T(8,128)} %bitcast.32, s32[1]{0:T(128)} %bitcast.5.tp_ref, bf16[64,64,256]{2,1,0:T(8,128)(2,1)} %all-to-all-done.2.came_ref), custom_call_target="tpu_custom_call" | custom-call | tf_op jit(solution)/shard_map/value_totals/pallas_call | solution.py:251
  121.0 8.9 %weight.1 = bf16[64,32,256]{2,1,0:T(8,128)(2,1)} custom-call(bf16[2048,2048]{1,0:T(8,128)(2,1)} %bitcast.27, bf16[256,2048]{1,0:T(8,128)(2,1)} %get-tuple-element.25.vt_ref), custom_call_target="tpu_custom_call" | custom-call | tf_op jit(solution)/shard_map/weight/pallas_call | solution.py:262
  130.0 10.7 %all-to-all-done.4.came_ref = bf16[64,64,256]{2,1,0:T(8,128)(2,1)} async-done(((bf16[64,64,256]{2,1,0:T(8,128)(2,1)}), bf16[64,64,256]{2,1,0:T(8,128)(2,1)}, u32[]{:S(2)}, u32[]{:S(2)}) %all-to-all-start.4) | async-done | bytes 2097184 | tf_op jit(solution)/shard_map/all_to_all | solution.py:29
  140.6 8.0 %all-to-all-start.5 = ((bf16[64,32,256]{2,1,0:T(8,128)(2,1)}), bf16[64,32,256]{2,1,0:T(8,128)(2,1)S(1)}, u32[]{:S(2)}, u32[]{:S(2)}) async-start(bf16[64,32,256]{2,1,0:T(8,128)(2,1)} %weight.1), calls=%async_computation.5 | async-start | bytes 2097152 | tf_op jit(solution)/shard_map/all_to_all | solution.py:29
  148.6 3.4 %back.3 = bf16[256,2048]{1,0:T(8,128)(2,1)} custom-call(bf16[256,256]{1,0:T(8,128)(2,1)} %get-tuple-element.38.refs_0_, bf16[256,256]{1,0:T(8,128)(2,1)} %get-tuple-element.39.refs_1_, bf16[2048,256]{1,0:T(8,128)(2,1)} %refs_2_.3, bf16[2048,256]{1,0:T(8,128)(2,1)} %refs_3_.3), custom_call_target="tpu_custom_call" | custom-call | tf_op jit(solution)/shard_map/back/pallas_call | solution.py:160
  152.0 3.6 %collective-permute-start.4 = (bf16[256,2048]{1,0:T(8,128)(2,1)}, bf16[256,2048]{1,0:T(8,128)(2,1)}, u32[]{:S(2)}, u32[]{:S(2)}) collective-permute-start(bf16[256,2048]{1,0:T(8,128)(2,1)} %back.3), channel_id=1, source_target_pairs={{0,1},{1,0},{2,3},{3,2},{4,5},{5,4},{6,7},{7,6},{8,9},{9,8},{10,11... | collective-permute-start | bytes 3145736 | tf_op jit(solution)/shard_map/ppermute | solution.py:25
  155.6 3.3 %key_totals.1 = (bf16[16,64,256]{2,1,0:T(8,128)(2,1)}, bf16[16,64,256]{2,1,0:T(8,128)(2,1)}) custom-call(s32[64,128]{1,0:T(8,128)} %bitcast.33, s32[1]{0:T(128)} %bitcast.5.tp_ref, bf16[64,64,256]{2,1,0:T(8,128)(2,1)} %all-to-all-done.4.came_ref), custom_call_target="tpu_custom_call" | custom-call | tf_op jit(solution)/shard_map/key_totals/pallas_call | solution.py:275
  158.9 7.5 %all-to-all-done.5 = bf16[64,32,256]{2,1,0:T(8,128)(2,1)S(1)} async-done(((bf16[64,32,256]{2,1,0:T(8,128)(2,1)}), bf16[64,32,256]{2,1,0:T(8,128)(2,1)S(1)}, u32[]{:S(2)}, u32[]{:S(2)}) %all-to-all-start.5) | async-done | bytes 1048608 | tf_op jit(solution)/shard_map/all_to_all | solution.py:29
  166.4 0.2 reduce_sum.12
  166.6 1.1 broadcast_in_dim.3
  167.7 4.8 %all-to-all-start.6 = ((bf16[64,32,256]{2,1,0:T(8,128)(2,1)}), bf16[64,32,256]{2,1,0:T(8,128)(2,1)S(1)}, u32[]{:S(2)}, u32[]{:S(2)}) async-start(bf16[64,32,256]{2,1,0:T(8,128)(2,1)} %broadcast_in_dim.3), calls=%async_computation.6 | async-start | bytes 2097152 | tf_op jit(solution)/shard_map/all_to_all | solution.py:29
  172.5 2.2 %collective-permute-start.3 = (bf16[1024,256]{1,0:T(8,128)(2,1)}, bf16[1024,256]{1,0:T(8,128)(2,1)}, u32[]{:S(2)}, u32[]{:S(2)}) collective-permute-start(bf16[1024,256]{1,0:T(8,128)(2,1)} %bitcast.41), channel_id=1, source_target_pairs={{0,1},{1,0},{2,3},{3,2},{4,5},{5,4},{6,7},{7,6},{8,9},{9,8},{10,11... | collective-permute-start | bytes 1572872 | tf_op jit(solution)/shard_map/ppermute | solution.py:25
  174.7 0.1 collective-permute-start.2
  174.8 3.7 %back.2.refs_8_ = f32[256,2048]{1,0:T(8,128)} custom-call(bf16[256,256]{1,0:T(8,128)(2,1)} %get-tuple-element.36.refs_0_, bf16[256,256]{1,0:T(8,128)(2,1)} %get-tuple-element.37.refs_1_, bf16[2048,256]{1,0:T(8,128)(2,1)} %refs_2_.3, bf16[2048,256]{1,0:T(8,128)(2,1)} %refs_3_.3), custom_call_target="tpu_custom_call" | custom-call | tf_op jit(solution)/shard_map/back/pallas_call | solution.py:160
  178.6 0.0 collective-permute-done.4.refs_9_
  178.6 0.0 collective-permute-done.3.refs_3_
  178.6 0.0 collective-permute-done.2.refs_1_
  178.6 9.6 %last.1 = (bf16[1024,2048]{1,0:T(8,128)(2,1)}, bf16[256,2048]{1,0:T(8,128)(2,1)}) custom-call(bf16[1024,256]{1,0:T(8,128)(2,1)} %bitcast.35, bf16[1024,256]{1,0:T(8,128)(2,1)} %collective-permute-done.2.refs_1_, bf16[1024,256]{1,0:T(8,128)(2,1)} %bitcast.34, bf16[1024,256]{1,0:T(8,128)(2,1)} %collective-permute-done.3.refs_3_, bf16[2048,256]{1,0:T(8,128)(2,1)} %refs_4_.1, ...), custom_call_target="tpu_custom_call" | custom-call | tf_op jit(solution)/shard_map/last/pallas_call | solution.py:183
  188.2 3.5 %all-to-all-done.6 = bf16[64,32,256]{2,1,0:T(8,128)(2,1)S(1)} async-done(((bf16[64,32,256]{2,1,0:T(8,128)(2,1)}), bf16[64,32,256]{2,1,0:T(8,128)(2,1)S(1)}, u32[]{:S(2)}, u32[]{:S(2)}) %all-to-all-start.6) | async-done | bytes 1048608 | tf_op jit(solution)/shard_map/all_to_all | solution.py:29
  191.7 1.5 bitcast_convert_fusion
Async XLA Ops:
  0.6 61.4 %copy-start = (bf16[512,2048]{1,0:T(8,128)(2,1)S(1)}, bf16[512,2048]{1,0:T(8,128)(2,1)}, u32[]{:S(2)}) copy-start(bf16[512,2048]{1,0:T(8,128)(2,1)} %param.8) | copy-start | bytes 6291460
  0.6 23.2 %collective-permute-start = (bf16[2048,256]{1,0:T(8,128)(2,1)}, bf16[2048,256]{1,0:T(8,128)(2,1)S(1)}, u32[]{:S(2)}, u32[]{:S(2)}) collective-permute-start(bf16[2048,256]{1,0:T(8,128)(2,1)} %refs_4_.1), channel_id=1, source_target_pairs={{0,1},{1,0},{2,3},{3,2},{4,5},{5,4},{6,7},{7,6},{8,9},{9,8},{10,11... | collective-permute-start | bytes 3145736 | tf_op jit(solution)/shard_map/ppermute | solution.py:25
  0.7 23.1 %collective-permute-start.1 = (bf16[2048,256]{1,0:T(8,128)(2,1)}, bf16[2048,256]{1,0:T(8,128)(2,1)}, u32[]{:S(2)}, u32[]{:S(2)}) collective-permute-start(bf16[2048,256]{1,0:T(8,128)(2,1)} %refs_6_.1), channel_id=1, source_target_pairs={{0,1},{1,0},{2,3},{3,2},{4,5},{5,4},{6,7},{7,6},{8,9},{9,8},{10,11... | collective-permute-start | bytes 3145736 | tf_op jit(solution)/shard_map/ppermute | solution.py:25
  2.8 21.0 %all-to-all-start = ((s32[64,1,128]{2,1,0:T(1,128)}), s32[64,1,128]{2,1,0:T(1,128)S(1)}, u32[]{:S(2)}, u32[]{:S(2)}) async-start(s32[64,1,128]{2,1,0:T(1,128)} %bitcast.36), calls=%async_computation | async-start | bytes 65536 | tf_op jit(solution)/shard_map/all_to_all | solution.py:29
  23.8 0.6 copy-start.5
  23.8 1.1 copy-start.3
  27.4 8.2 %copy-start.4 = (bf16[2048,256]{1,0:T(8,128)(2,1)S(1)}, bf16[2048,256]{1,0:T(8,128)(2,1)}, u32[]{:S(2)}) copy-start(bf16[2048,256]{1,0:T(8,128)(2,1)} %refs_6_.1) | copy-start | bytes 3145732
  27.4 29.0 %all-to-all-start.1 = ((bf16[64,64,256]{2,1,0:T(8,128)(2,1)}), bf16[64,64,256]{2,1,0:T(8,128)(2,1)}, u32[]{:S(2)}, u32[]{:S(2)}) async-start(bf16[64,64,256]{2,1,0:T(8,128)(2,1)} %pick.2), calls=%async_computation.1 | async-start | bytes 4194304 | tf_op jit(solution)/shard_map/all_to_all | solution.py:29
  44.9 17.1 %copy-start.1 = (bf16[2048,256]{1,0:T(8,128)(2,1)S(1)}, bf16[2048,256]{1,0:T(8,128)(2,1)}, u32[]{:S(2)}) copy-start(bf16[2048,256]{1,0:T(8,128)(2,1)} %refs_2_.3) | copy-start | bytes 3145732
  56.4 26.4 %all-to-all-start.3 = ((bf16[64,64,256]{2,1,0:T(8,128)(2,1)}), bf16[64,64,256]{2,1,0:T(8,128)(2,1)}, u32[]{:S(2)}, u32[]{:S(2)}) async-start(bf16[64,64,256]{2,1,0:T(8,128)(2,1)} %pick.3), calls=%async_computation.3 | async-start | bytes 4194304 | tf_op jit(solution)/shard_map/all_to_all | solution.py:29
  62.0 1.5 copy-start.2
  62.0 1.4 copy-start.6
  82.8 26.8 %all-to-all-start.2 = ((bf16[64,64,256]{2,1,0:T(8,128)(2,1)}), bf16[64,64,256]{2,1,0:T(8,128)(2,1)}, u32[]{:S(2)}, u32[]{:S(2)}) async-start(bf16[64,64,256]{2,1,0:T(8,128)(2,1)} %get-tuple-element.24), calls=%async_computation.2 | async-start | bytes 4194304 | tf_op jit(solution)/shard_map/all_to_all | solution.py:29
  109.6 31.0 %all-to-all-start.4 = ((bf16[64,64,256]{2,1,0:T(8,128)(2,1)}), bf16[64,64,256]{2,1,0:T(8,128)(2,1)}, u32[]{:S(2)}, u32[]{:S(2)}) async-start(bf16[64,64,256]{2,1,0:T(8,128)(2,1)} %get-tuple-element.27), calls=%async_computation.4 | async-start | bytes 4194304 | tf_op jit(solution)/shard_map/all_to_all | solution.py:29
  140.6 25.8 %all-to-all-start.5 = ((bf16[64,32,256]{2,1,0:T(8,128)(2,1)}), bf16[64,32,256]{2,1,0:T(8,128)(2,1)S(1)}, u32[]{:S(2)}, u32[]{:S(2)}) async-start(bf16[64,32,256]{2,1,0:T(8,128)(2,1)} %weight.1), calls=%async_computation.5 | async-start | bytes 2097152 | tf_op jit(solution)/shard_map/all_to_all | solution.py:29
  152.0 26.6 %collective-permute-start.4 = (bf16[256,2048]{1,0:T(8,128)(2,1)}, bf16[256,2048]{1,0:T(8,128)(2,1)}, u32[]{:S(2)}, u32[]{:S(2)}) collective-permute-start(bf16[256,2048]{1,0:T(8,128)(2,1)} %back.3), channel_id=1, source_target_pairs={{0,1},{1,0},{2,3},{3,2},{4,5},{5,4},{6,7},{7,6},{8,9},{9,8},{10,11... | collective-permute-start | bytes 3145736 | tf_op jit(solution)/shard_map/ppermute | solution.py:25
  167.7 24.1 %all-to-all-start.6 = ((bf16[64,32,256]{2,1,0:T(8,128)(2,1)}), bf16[64,32,256]{2,1,0:T(8,128)(2,1)S(1)}, u32[]{:S(2)}, u32[]{:S(2)}) async-start(bf16[64,32,256]{2,1,0:T(8,128)(2,1)} %broadcast_in_dim.3), calls=%async_computation.6 | async-start | bytes 2097152 | tf_op jit(solution)/shard_map/all_to_all | solution.py:29
  172.5 6.1 %collective-permute-start.3 = (bf16[1024,256]{1,0:T(8,128)(2,1)}, bf16[1024,256]{1,0:T(8,128)(2,1)}, u32[]{:S(2)}, u32[]{:S(2)}) collective-permute-start(bf16[1024,256]{1,0:T(8,128)(2,1)} %bitcast.41), channel_id=1, source_target_pairs={{0,1},{1,0},{2,3},{3,2},{4,5},{5,4},{6,7},{7,6},{8,9},{9,8},{10,11... | collective-permute-start | bytes 1572872 | tf_op jit(solution)/shard_map/ppermute | solution.py:25
  174.7 3.8 %collective-permute-start.2 = (bf16[1024,256]{1,0:T(8,128)(2,1)}, bf16[1024,256]{1,0:T(8,128)(2,1)}, u32[]{:S(2)}, u32[]{:S(2)}) collective-permute-start(bf16[1024,256]{1,0:T(8,128)(2,1)} %bitcast.42), channel_id=1, source_target_pairs={{0,1},{1,0},{2,3},{3,2},{4,5},{5,4},{6,7},{7,6},{8,9},{9,8},{10,11... | collective-permute-start | bytes 1572872 | tf_op jit(solution)/shard_map/ppermute | solution.py:25
where the time goes:
time: 196 us; the launch traced here: 193 us
  waiting for transfers between devices  62.5 us (32%)
  starting transfers between devices  57 us (29%)
  Pallas kernels  52.4 us (27%)
  matrix products  16.7 us (9%)
  local copies, waits for them, and re-layouts  2.2 us (1%)
    all_to_all x7, waiting for transfers between devices, exchange(): return lax.all_to_all(x, 'st', split_axis=0, concat_axis=0, tiled=True)  62.5 us
    all_to_all x7, starting transfers between devices, exchange(): return lax.all_to_all(x, 'st', split_axis=0, concat_axis=0, tiled=True)  50.5 us
    pallas_call x1, Pallas kernels, back_and_add(): pl.pallas_call(functools.partial(last_kernel, len(terms)), grid=(steps,),...  9.58 us
    pallas_call x1, Pallas kernels, body(): pl.pallas_call(weight_kernel, grid=(depth // tile,), out_shape=jax.ShapeD...  8.93 us
    pallas_call x2, Pallas kernels, back(): pl.pallas_call(functools.partial(back_kernel, len(terms)), grid=(rows //...  7.14 us
    dot_general x1, matrix products, body(): jnp.dot(store_rows, key_weight, preferred_element_type=F32).astype(BF16)  6.93 us
    pallas_call x1, Pallas kernels, body(): pl.pallas_call(functools.partial(grads_kernel, held), out_shape=(half_tok...  6.77 us
    dot_general x1, matrix products, body(): jnp.dot(store_rows, value_weight, preferred_element_type=F32).astype(BF16)  6.7 us
  transfers between devices with their start and end apart: 12, of which 7 were waited for; matrix products, arithmetic and copies ran while one was open for 9% of the time, Pallas kernels for 26%

commit v1 on v0

--- a/solution.py
+++ b/solution.py
@@ -8,8 +8,7 @@
 from jax.sharding import PartitionSpec as P
 
 HEAD_DIM = 256
-PAUSE = 2650
-PAUSE_AGAIN = 1300
+PAUSE = 2900
 F32 = jnp.float32
 BF16 = jnp.bfloat16
 VMEM = pl.BlockSpec(memory_space=pltpu.VMEM)
@@ -216,7 +215,7 @@
     pause = tp * PAUSE
     came_keys = exchange(pick(wanted, pause, keys, other_key, other_value))
     values = jnp.dot(store_rows, value_weight, preferred_element_type=F32).astype(BF16).reshape(held, span, width)
-    came_values = exchange(pick(wanted, tp * PAUSE_AGAIN, values))
+    came_values = exchange(pick(wanted, jnp.zeros_like(tp), values))
 
     queries = jnp.dot(hidden, query_weight, preferred_element_type=F32).astype(BF16)
     gates = jnp.dot(hidden, gate_weight, preferred_element_type=F32)

time: 196 us -> 191 us (0.974)
  waiting for transfers between devices: 62.5 us -> 51 us
  starting transfers between devices: 57 us -> 63.2 us
    all_to_all x7, waiting for transfers between devices: 62.5 us -> 51 us  [exchange(): return lax.all_to_all(x, 'st', split_axis=0, concat_axis=0, tiled=True)]
    ppermute x5, starting transfers between devices: 6.5 us -> 10.4 us  [swap_tp(): return lax.ppermute(x, 'tp', [(0, 1), (1, 0)])]
    all_to_all x7, starting transfers between devices: 50.5 us -> 52.8 us  [exchange(): return lax.all_to_all(x, 'st', split_axis=0, concat_axis=0, tiled=True)]
  transfers between devices with their start and end apart: 12 -> 12, of which waited for: 7 -> 6; matrix products, arithmetic and copies ran while one was open for 9% -> 10% of each run, Pallas kernels for 26% -> 27%
where the time goes in v1:
time: 191 us; the launch traced here: 188 us
  starting transfers between devices  63.2 us (33%)
  Pallas kernels  52.4 us (27%)
  waiting for transfers between devices  51 us (27%)
  matrix products  16.7 us (9%)
  local copies, waits for them, and re-layouts  2.2 us (1%)
    all_to_all x7, starting transfers between devices, exchange(): return lax.all_to_all(x, 'st', split_axis=0, concat_axis=0, tiled=True)  52.8 us
    all_to_all x7, waiting for transfers between devices, exchange(): return lax.all_to_all(x, 'st', split_axis=0, concat_axis=0, tiled=True)  51 us
    ppermute x5, starting transfers between devices, swap_tp(): return lax.ppermute(x, 'tp', [(0, 1), (1, 0)])  10.4 us
    pallas_call x1, Pallas kernels, back_and_add(): pl.pallas_call(functools.partial(last_kernel, len(terms)), grid=(steps,),...  9.58 us
    pallas_call x1, Pallas kernels, body(): pl.pallas_call(weight_kernel, grid=(depth // tile,), out_shape=jax.ShapeD...  8.93 us
    pallas_call x2, Pallas kernels, back(): pl.pallas_call(functools.partial(back_kernel, len(terms)), grid=(rows //...  7.14 us
    dot_general x1, matrix products, body(): jnp.dot(store_rows, key_weight, preferred_element_type=F32).astype(BF16)  6.93 us
    pallas_call x1, Pallas kernels, body(): pl.pallas_call(functools.partial(grads_kernel, held), out_shape=(half_tok...  6.77 us
  transfers between devices with their start and end apart: 12, of which 6 were waited for; matrix products, arithmetic and copies ran while one was open for 10% of the time, Pallas kernels for 27%

profile of v1, /device:TPU:0, one launch (start us, length us, event | category | flops | bytes accessed | tf_op | source)
XLA Modules:
  0.0 188.0 jit_solution(12728764076706297787)
XLA Ops:
  0.6 0.0 copy-start
  0.6 0.1 collective-permute-start
  0.7 0.5 collective-permute-start.1
  1.2 1.5 request.1
  2.8 11.5 %all-to-all-start = ((s32[64,1,128]{2,1,0:T(1,128)}), s32[64,1,128]{2,1,0:T(1,128)S(1)}, u32[]{:S(2)}, u32[]{:S(2)}) async-start(s32[64,1,128]{2,1,0:T(1,128)} %bitcast.36), calls=%async_computation | async-start | bytes 65536 | tf_op jit(solution)/shard_map/all_to_all | solution.py:28
  14.3 6.9 %convolution_convert_fusion.1 = bf16[2048,256]{1,0:T(8,128)(2,1)} fusion(bf16[2048,2048]{1,0:T(8,128)(2,1)} %bitcast.25, bf16[2048,256]{1,0:T(8,128)(2,1)} %refs_4_.1), kind=kOutput, calls=%fused_computation.1 | convolution fusion | flops 2148007936 | bytes 10485760 | tf_op jit(solution)/shard_map/dot_general | solution.py:214
  21.2 2.6 %all-to-all-done = s32[64,1,128]{2,1,0:T(1,128)S(1)} async-done(((s32[64,1,128]{2,1,0:T(1,128)}), s32[64,1,128]{2,1,0:T(1,128)S(1)}, u32[]{:S(2)}, u32[]{:S(2)}) %all-to-all-start) | async-done | bytes 32800 | tf_op jit(solution)/shard_map/all_to_all | solution.py:28
  23.8 0.0 copy-start.5
  23.8 0.0 collective-permute-done.refs_0_.refs_5_
  23.8 0.0 copy-start.3
  23.8 0.0 collective-permute-done.1.refs_1_.refs_7_
  23.8 0.6 copy-done.5
  24.4 0.5 copy-done.3
  24.9 2.5 %pick.2 = bf16[64,64,256]{2,1,0:T(8,128)(2,1)} custom-call(s32[64,128]{1,0:T(8,128)} %bitcast.30, s32[1]{0:T(128)S(6)} %mul.11.pause_ref, bf16[32,64,256]{2,1,0:T(8,128)(2,1)} %bitcast.29, bf16[2048,256]{1,0:T(8,128)(2,1)} %copy-done.3, bf16[2048,256]{1,0:T(8,128)(2,1)} %collective-permute-done.1.refs_1_.refs_7_), custom_call_target="tpu_custom_call" | custom-call | tf_op jit(solution)/shard_map/pick/pallas_call | solution.py:56
  27.4 0.0 copy-start.4
  27.4 8.2 %all-to-all-start.1 = ((bf16[64,64,256]{2,1,0:T(8,128)(2,1)}), bf16[64,64,256]{2,1,0:T(8,128)(2,1)}, u32[]{:S(2)}, u32[]{:S(2)}) async-start(bf16[64,64,256]{2,1,0:T(8,128)(2,1)} %pick.2), calls=%async_computation.1 | async-start | bytes 4194304 | tf_op jit(solution)/shard_map/all_to_all | solution.py:28
  35.6 0.0 copy-done.4
  35.6 6.7 %convolution_convert_fusion = bf16[2048,256]{1,0:T(8,128)(2,1)} fusion(bf16[2048,2048]{1,0:T(8,128)(2,1)} %bitcast.26, bf16[2048,256]{1,0:T(8,128)(2,1)S(1)} %copy-done.4), kind=kOutput, calls=%fused_computation | convolution fusion | flops 2148007936 | bytes 10485760 | tf_op jit(solution)/shard_map/dot_general | solution.py:217
  42.3 2.5 %pick.3 = bf16[64,64,256]{2,1,0:T(8,128)(2,1)} custom-call(s32[64,128]{1,0:T(8,128)} %bitcast.31, s32[1]{0:T(128)} %constant.4.clone.1.pause_ref, bf16[32,64,256]{2,1,0:T(8,128)(2,1)} %bitcast.28), custom_call_target="tpu_custom_call" | custom-call | tf_op jit(solution)/shard_map/pick/pallas_call | solution.py:56
  44.9 0.0 copy-start.1
  44.9 10.9 %all-to-all-done.1.k_ref = bf16[64,64,256]{2,1,0:T(8,128)(2,1)} async-done(((bf16[64,64,256]{2,1,0:T(8,128)(2,1)}), bf16[64,64,256]{2,1,0:T(8,128)(2,1)}, u32[]{:S(2)}, u32[]{:S(2)}) %all-to-all-start.1) | async-done | bytes 2097184 | tf_op jit(solution)/shard_map/all_to_all | solution.py:28
  55.8 5.6 %all-to-all-start.3 = ((bf16[64,64,256]{2,1,0:T(8,128)(2,1)}), bf16[64,64,256]{2,1,0:T(8,128)(2,1)}, u32[]{:S(2)}, u32[]{:S(2)}) async-start(bf16[64,64,256]{2,1,0:T(8,128)(2,1)} %pick.3), calls=%async_computation.3 | async-start | bytes 4194304 | tf_op jit(solution)/shard_map/all_to_all | solution.py:28
  61.4 0.0 copy-done
  61.4 0.0 copy-done.1
  61.4 0.0 copy-start.2
  61.4 0.0 copy-start.6
  61.4 1.4 convolution_convert_fusion.2.q_ref
  62.9 0.0 copy-done.2
  62.9 0.0 copy-done.6
  62.9 1.6 multiply_convert_fusion
  64.5 5.4 %probs.1 = (f32[512,256]{1,0:T(8,128)}, bf16[64,64,256]{2,1,0:T(8,128)(2,1)}) custom-call(s32[4,8]{1,0:T(4,128)} %bitcast.38, bf16[512,256]{1,0:T(8,128)(2,1)} %convolution_convert_fusion.2.q_ref, bf16[512,256]{1,0:T(8,128)(2,1)} %get-tuple-element.45.da_ref, bf16[64,64,256]{2,1,0:T(8,128)(2,1)} %all-to-all-done.1.k_ref), custom_call_target="tpu_custom_call" | custom-call | tf_op jit(solution)/shard_map/probs/pallas_call | solution.py:224
  69.9 11.7 %all-to-all-done.3.v_ref = bf16[64,64,256]{2,1,0:T(8,128)(2,1)} async-done(((bf16[64,64,256]{2,1,0:T(8,128)(2,1)}), bf16[64,64,256]{2,1,0:T(8,128)(2,1)}, u32[]{:S(2)}, u32[]{:S(2)}) %all-to-all-start.3) | async-done | bytes 2097184 | tf_op jit(solution)/shard_map/all_to_all | solution.py:28
  81.6 5.7 %all-to-all-start.2 = ((bf16[64,64,256]{2,1,0:T(8,128)(2,1)}), bf16[64,64,256]{2,1,0:T(8,128)(2,1)}, u32[]{:S(2)}, u32[]{:S(2)}) async-start(bf16[64,64,256]{2,1,0:T(8,128)(2,1)} %get-tuple-element.24), calls=%async_computation.2 | async-start | bytes 4194304 | tf_op jit(solution)/shard_map/all_to_all | solution.py:28
  87.3 6.8 %grads.1 = (bf16[256,256]{1,0:T(8,128)(2,1)}, bf16[256,256]{1,0:T(8,128)(2,1)}, bf16[256,256]{1,0:T(8,128)(2,1)}, bf16[256,256]{1,0:T(8,128)(2,1)}, bf16[64,64,256]{2,1,0:T(8,128)(2,1)}) custom-call(s32[4,8]{1,0:T(4,128)} %bitcast.39, s32[1]{0:T(128)} %bitcast.5.tp_ref, bf16[512,256]{1,0:T(8,128)(2,1)} %convolution_convert_fusion.2.q_ref, ...), custom_call_target="tpu_custom_call" | custom-call | tf_op jit(solution)/shard_map/grads/pallas_call | solution.py:238
  94.1 13.2 %all-to-all-done.2.came_ref = bf16[64,64,256]{2,1,0:T(8,128)(2,1)} async-done(((bf16[64,64,256]{2,1,0:T(8,128)(2,1)}), bf16[64,64,256]{2,1,0:T(8,128)(2,1)}, u32[]{:S(2)}, u32[]{:S(2)}) %all-to-all-start.2) | async-done | bytes 2097184 | tf_op jit(solution)/shard_map/all_to_all | solution.py:28
  107.3 5.6 %all-to-all-start.4 = ((bf16[64,64,256]{2,1,0:T(8,128)(2,1)}), bf16[64,64,256]{2,1,0:T(8,128)(2,1)}, u32[]{:S(2)}, u32[]{:S(2)}) async-start(bf16[64,64,256]{2,1,0:T(8,128)(2,1)} %get-tuple-element.27), calls=%async_computation.4 | async-start | bytes 4194304 | tf_op jit(solution)/shard_map/all_to_all | solution.py:28
  112.9 4.7 %value_totals.1 = (bf16[16,64,256]{2,1,0:T(8,128)(2,1)}, bf16[16,64,256]{2,1,0:T(8,128)(2,1)}, bf16[256,2048]{1,0:T(8,128)(2,1)}) custom-call(s32[64,128]{1,0:T(8,128)} %bitcast.32, s32[1]{0:T(128)} %bitcast.5.tp_ref, bf16[64,64,256]{2,1,0:T(8,128)(2,1)} %all-to-all-done.2.came_ref), custom_call_target="tpu_custom_call" | custom-call | tf_op jit(solution)/shard_map/value_totals/pallas_call | solution.py:250
  117.6 8.9 %weight.1 = bf16[64,32,256]{2,1,0:T(8,128)(2,1)} custom-call(bf16[2048,2048]{1,0:T(8,128)(2,1)} %bitcast.27, bf16[256,2048]{1,0:T(8,128)(2,1)} %get-tuple-element.25.vt_ref), custom_call_target="tpu_custom_call" | custom-call | tf_op jit(solution)/shard_map/weight/pallas_call | solution.py:261
  126.6 7.8 %all-to-all-done.4.came_ref = bf16[64,64,256]{2,1,0:T(8,128)(2,1)} async-done(((bf16[64,64,256]{2,1,0:T(8,128)(2,1)}), bf16[64,64,256]{2,1,0:T(8,128)(2,1)}, u32[]{:S(2)}, u32[]{:S(2)}) %all-to-all-start.4) | async-done | bytes 2097184 | tf_op jit(solution)/shard_map/all_to_all | solution.py:28
  134.4 6.2 %all-to-all-start.5 = ((bf16[64,32,256]{2,1,0:T(8,128)(2,1)}), bf16[64,32,256]{2,1,0:T(8,128)(2,1)S(1)}, u32[]{:S(2)}, u32[]{:S(2)}) async-start(bf16[64,32,256]{2,1,0:T(8,128)(2,1)} %weight.1), calls=%async_computation.5 | async-start | bytes 2097152 | tf_op jit(solution)/shard_map/all_to_all | solution.py:28
  140.6 3.4 %back.3 = bf16[256,2048]{1,0:T(8,128)(2,1)} custom-call(bf16[256,256]{1,0:T(8,128)(2,1)} %get-tuple-element.38.refs_0_, bf16[256,256]{1,0:T(8,128)(2,1)} %get-tuple-element.39.refs_1_, bf16[2048,256]{1,0:T(8,128)(2,1)} %refs_2_.3, bf16[2048,256]{1,0:T(8,128)(2,1)} %refs_3_.3), custom_call_target="tpu_custom_call" | custom-call | tf_op jit(solution)/shard_map/back/pallas_call | solution.py:159
  144.0 8.2 %collective-permute-start.4 = (bf16[256,2048]{1,0:T(8,128)(2,1)}, bf16[256,2048]{1,0:T(8,128)(2,1)}, u32[]{:S(2)}, u32[]{:S(2)}) collective-permute-start(bf16[256,2048]{1,0:T(8,128)(2,1)} %back.3), channel_id=1, source_target_pairs={{0,1},{1,0},{2,3},{3,2},{4,5},{5,4},{6,7},{7,6},{8,9},{9,8},{10,11... | collective-permute-start | bytes 3145736 | tf_op jit(solution)/shard_map/ppermute | solution.py:24
  152.2 3.3 %key_totals.1 = (bf16[16,64,256]{2,1,0:T(8,128)(2,1)}, bf16[16,64,256]{2,1,0:T(8,128)(2,1)}) custom-call(s32[64,128]{1,0:T(8,128)} %bitcast.33, s32[1]{0:T(128)} %bitcast.5.tp_ref, bf16[64,64,256]{2,1,0:T(8,128)(2,1)} %all-to-all-done.4.came_ref), custom_call_target="tpu_custom_call" | custom-call | tf_op jit(solution)/shard_map/key_totals/pallas_call | solution.py:274
  155.5 0.0 all-to-all-done.5
  155.5 0.2 reduce_sum.12
  155.7 1.1 broadcast_in_dim.3
  156.8 10.0 %all-to-all-start.6 = ((bf16[64,32,256]{2,1,0:T(8,128)(2,1)}), bf16[64,32,256]{2,1,0:T(8,128)(2,1)S(1)}, u32[]{:S(2)}, u32[]{:S(2)}) async-start(bf16[64,32,256]{2,1,0:T(8,128)(2,1)} %broadcast_in_dim.3), calls=%async_computation.6 | async-start | bytes 2097152 | tf_op jit(solution)/shard_map/all_to_all | solution.py:28
  166.8 1.5 collective-permute-start.3
  168.3 0.1 collective-permute-start.2
  168.4 3.7 %back.2.refs_8_ = f32[256,2048]{1,0:T(8,128)} custom-call(bf16[256,256]{1,0:T(8,128)(2,1)} %get-tuple-element.36.refs_0_, bf16[256,256]{1,0:T(8,128)(2,1)} %get-tuple-element.37.refs_1_, bf16[2048,256]{1,0:T(8,128)(2,1)} %refs_2_.3, bf16[2048,256]{1,0:T(8,128)(2,1)} %refs_3_.3), custom_call_target="tpu_custom_call" | custom-call | tf_op jit(solution)/shard_map/back/pallas_call | solution.py:159
  172.2 0.0 collective-permute-done.4.refs_9_
  172.2 0.0 collective-permute-done.3.refs_3_
  172.2 0.0 collective-permute-done.2.refs_1_
  172.2 9.6 %last.1 = (bf16[1024,2048]{1,0:T(8,128)(2,1)}, bf16[256,2048]{1,0:T(8,128)(2,1)}) custom-call(bf16[1024,256]{1,0:T(8,128)(2,1)} %bitcast.35, bf16[1024,256]{1,0:T(8,128)(2,1)} %collective-permute-done.2.refs_1_, bf16[1024,256]{1,0:T(8,128)(2,1)} %bitcast.34, bf16[1024,256]{1,0:T(8,128)(2,1)} %collective-permute-done.3.refs_3_, bf16[2048,256]{1,0:T(8,128)(2,1)} %refs_4_.1, ...), custom_call_target="tpu_custom_call" | custom-call | tf_op jit(solution)/shard_map/last/pallas_call | solution.py:182
  181.8 4.7 %all-to-all-done.6 = bf16[64,32,256]{2,1,0:T(8,128)(2,1)S(1)} async-done(((bf16[64,32,256]{2,1,0:T(8,128)(2,1)}), bf16[64,32,256]{2,1,0:T(8,128)(2,1)S(1)}, u32[]{:S(2)}, u32[]{:S(2)}) %all-to-all-start.6) | async-done | bytes 1048608 | tf_op jit(solution)/shard_map/all_to_all | solution.py:28
  186.5 1.5 bitcast_convert_fusion
Async XLA Ops:
  0.6 60.7 %copy-start = (bf16[512,2048]{1,0:T(8,128)(2,1)S(1)}, bf16[512,2048]{1,0:T(8,128)(2,1)}, u32[]{:S(2)}) copy-start(bf16[512,2048]{1,0:T(8,128)(2,1)} %param.8) | copy-start | bytes 6291460
  0.6 23.2 %collective-permute-start = (bf16[2048,256]{1,0:T(8,128)(2,1)}, bf16[2048,256]{1,0:T(8,128)(2,1)S(1)}, u32[]{:S(2)}, u32[]{:S(2)}) collective-permute-start(bf16[2048,256]{1,0:T(8,128)(2,1)} %refs_4_.1), channel_id=1, source_target_pairs={{0,1},{1,0},{2,3},{3,2},{4,5},{5,4},{6,7},{7,6},{8,9},{9,8},{10,11... | collective-permute-start | bytes 3145736 | tf_op jit(solution)/shard_map/ppermute | solution.py:24
  0.7 23.1 %collective-permute-start.1 = (bf16[2048,256]{1,0:T(8,128)(2,1)}, bf16[2048,256]{1,0:T(8,128)(2,1)}, u32[]{:S(2)}, u32[]{:S(2)}) collective-permute-start(bf16[2048,256]{1,0:T(8,128)(2,1)} %refs_6_.1), channel_id=1, source_target_pairs={{0,1},{1,0},{2,3},{3,2},{4,5},{5,4},{6,7},{7,6},{8,9},{9,8},{10,11... | collective-permute-start | bytes 3145736 | tf_op jit(solution)/shard_map/ppermute | solution.py:24
  2.8 21.0 %all-to-all-start = ((s32[64,1,128]{2,1,0:T(1,128)}), s32[64,1,128]{2,1,0:T(1,128)S(1)}, u32[]{:S(2)}, u32[]{:S(2)}) async-start(s32[64,1,128]{2,1,0:T(1,128)} %bitcast.36), calls=%async_computation | async-start | bytes 65536 | tf_op jit(solution)/shard_map/all_to_all | solution.py:28
  23.8 0.6 copy-start.5
  23.8 1.1 copy-start.3
  27.4 8.2 %copy-start.4 = (bf16[2048,256]{1,0:T(8,128)(2,1)S(1)}, bf16[2048,256]{1,0:T(8,128)(2,1)}, u32[]{:S(2)}) copy-start(bf16[2048,256]{1,0:T(8,128)(2,1)} %refs_6_.1) | copy-start | bytes 3145732
  27.4 28.4 %all-to-all-start.1 = ((bf16[64,64,256]{2,1,0:T(8,128)(2,1)}), bf16[64,64,256]{2,1,0:T(8,128)(2,1)}, u32[]{:S(2)}, u32[]{:S(2)}) async-start(bf16[64,64,256]{2,1,0:T(8,128)(2,1)} %pick.2), calls=%async_computation.1 | async-start | bytes 4194304 | tf_op jit(solution)/shard_map/all_to_all | solution.py:28
  44.9 16.5 %copy-start.1 = (bf16[2048,256]{1,0:T(8,128)(2,1)S(1)}, bf16[2048,256]{1,0:T(8,128)(2,1)}, u32[]{:S(2)}) copy-start(bf16[2048,256]{1,0:T(8,128)(2,1)} %refs_2_.3) | copy-start | bytes 3145732
  55.8 25.8 %all-to-all-start.3 = ((bf16[64,64,256]{2,1,0:T(8,128)(2,1)}), bf16[64,64,256]{2,1,0:T(8,128)(2,1)}, u32[]{:S(2)}, u32[]{:S(2)}) async-start(bf16[64,64,256]{2,1,0:T(8,128)(2,1)} %pick.3), calls=%async_computation.3 | async-start | bytes 4194304 | tf_op jit(solution)/shard_map/all_to_all | solution.py:28
  61.4 1.5 copy-start.2
  61.4 1.4 copy-start.6
  81.6 25.8 %all-to-all-start.2 = ((bf16[64,64,256]{2,1,0:T(8,128)(2,1)}), bf16[64,64,256]{2,1,0:T(8,128)(2,1)}, u32[]{:S(2)}, u32[]{:S(2)}) async-start(bf16[64,64,256]{2,1,0:T(8,128)(2,1)} %get-tuple-element.24), calls=%async_computation.2 | async-start | bytes 4194304 | tf_op jit(solution)/shard_map/all_to_all | solution.py:28
  107.3 27.0 %all-to-all-start.4 = ((bf16[64,64,256]{2,1,0:T(8,128)(2,1)}), bf16[64,64,256]{2,1,0:T(8,128)(2,1)}, u32[]{:S(2)}, u32[]{:S(2)}) async-start(bf16[64,64,256]{2,1,0:T(8,128)(2,1)} %get-tuple-element.27), calls=%async_computation.4 | async-start | bytes 4194304 | tf_op jit(solution)/shard_map/all_to_all | solution.py:28
  134.4 21.2 %all-to-all-start.5 = ((bf16[64,32,256]{2,1,0:T(8,128)(2,1)}), bf16[64,32,256]{2,1,0:T(8,128)(2,1)S(1)}, u32[]{:S(2)}, u32[]{:S(2)}) async-start(bf16[64,32,256]{2,1,0:T(8,128)(2,1)} %weight.1), calls=%async_computation.5 | async-start | bytes 2097152 | tf_op jit(solution)/shard_map/all_to_all | solution.py:28
  144.0 28.2 %collective-permute-start.4 = (bf16[256,2048]{1,0:T(8,128)(2,1)}, bf16[256,2048]{1,0:T(8,128)(2,1)}, u32[]{:S(2)}, u32[]{:S(2)}) collective-permute-start(bf16[256,2048]{1,0:T(8,128)(2,1)} %back.3), channel_id=1, source_target_pairs={{0,1},{1,0},{2,3},{3,2},{4,5},{5,4},{6,7},{7,6},{8,9},{9,8},{10,11... | collective-permute-start | bytes 3145736 | tf_op jit(solution)/shard_map/ppermute | solution.py:24
  156.8 29.7 %all-to-all-start.6 = ((bf16[64,32,256]{2,1,0:T(8,128)(2,1)}), bf16[64,32,256]{2,1,0:T(8,128)(2,1)S(1)}, u32[]{:S(2)}, u32[]{:S(2)}) async-start(bf16[64,32,256]{2,1,0:T(8,128)(2,1)} %broadcast_in_dim.3), calls=%async_computation.6 | async-start | bytes 2097152 | tf_op jit(solution)/shard_map/all_to_all | solution.py:28
  166.8 5.4 %collective-permute-start.3 = (bf16[1024,256]{1,0:T(8,128)(2,1)}, bf16[1024,256]{1,0:T(8,128)(2,1)}, u32[]{:S(2)}, u32[]{:S(2)}) collective-permute-start(bf16[1024,256]{1,0:T(8,128)(2,1)} %bitcast.41), channel_id=1, source_target_pairs={{0,1},{1,0},{2,3},{3,2},{4,5},{5,4},{6,7},{7,6},{8,9},{9,8},{10,11... | collective-permute-start | bytes 1572872 | tf_op jit(solution)/shard_map/ppermute | solution.py:24
  168.3 3.8 %collective-permute-start.2 = (bf16[1024,256]{1,0:T(8,128)(2,1)}, bf16[1024,256]{1,0:T(8,128)(2,1)}, u32[]{:S(2)}, u32[]{:S(2)}) collective-permute-start(bf16[1024,256]{1,0:T(8,128)(2,1)} %bitcast.42), channel_id=1, source_target_pairs={{0,1},{1,0},{2,3},{3,2},{4,5},{5,4},{6,7},{7,6},{8,9},{9,8},{10,11... | collective-permute-start | bytes 1572872 | tf_op jit(solution)/shard_map/ppermute | solution.py:24
